TPU v7x, 32 devices: a whole 2x2x4 slice. The times are simulated.
32 devices in a mesh: rep: 2 (over x), fs: 8 (over z, y), tp: 2 (over core).
Axes of the slice: x: 2, y: 2, z: 4, core: 2. Of those that a mesh axis runs over, the one named last changes fastest.
Arguments:
- inputs: bfloat16 [8192, 1024], P(('rep', 'fs', 'tp')), may hold values from -6 to 6
- up_proj: bfloat16 [1024, 4096], P('fs', 'tp'), may hold values from -0.1875 to 0.1875
- down_proj: bfloat16 [4096, 1024], P('tp', 'fs'), may hold values from -0.09375 to 0.09375
- out_cotangent: bfloat16 [8192, 1024], P(('rep', 'fs', 'tp')), may hold values from -6 to 6
Outputs:
- grad_inputs: bfloat16 [8192, 1024], P(('rep', 'fs', 'tp'))
- grad_up: float32 [1024, 4096], P('fs', 'tp')
- grad_down: float32 [4096, 1024], P('tp', 'fs')
- energy_up: float32 [1024], P('fs')
- energy_down: float32 [4096], P('tp')
All inputs are finite; a program needn't handle non-finite values.
Results may differ from a plain program's by a relative error of at most 0.001.
Values may be sent and summed in bfloat16 or wider, within the bound.
A program may use at most 128 MiB of HBM per device.

v0:
```python
import jax
import jax.numpy as jnp
from jax import lax
from jax.sharding import PartitionSpec as P

D = 1024
FF = 4096


def taken_in(shard, axis, dim, absorb, state):
    everything = jax.tree.map(lambda a: lax.all_gather(a, axis, axis=dim, tiled=True), shard)
    return absorb(state, everything, jnp.int32(0))


def summed_rows(product, span, axis):
    whole = product(jnp.int32(0), span * lax.axis_size(axis))
    return lax.psum_scatter(whole, axis, scatter_dimension=0, tiled=True)


def contract(left, right, left_dim, right_dim):
    return lax.dot_general(
        left, right, (((left_dim,), (right_dim,)), ((), ())), preferred_element_type=jnp.float32
    )


def body(inputs, up_proj, down_proj, out_cotangent):
    factor = float(
        inputs.shape[0] * lax.axis_size("rep") * lax.axis_size("fs") * lax.axis_size("tp")
    ) ** (-0.5)
    all_inputs, all_cotangent = (
        lax.all_gather(inputs, "tp", axis=0, tiled=True),
        lax.all_gather(out_cotangent, "tp", axis=0, tiled=True),
    )
    hidden_cols = up_proj.shape[1]
    group_rows = all_inputs.shape[0]
    whole_up = lax.all_gather(up_proj, "fs", axis=0, tiled=True)
    pre = jnp.dot(all_inputs, whole_up, preferred_element_type=jnp.float32)
    active = jnp.square(jax.nn.relu(pre)).astype(jnp.bfloat16)

    def add_cols(total, piece, start):
        columns = lax.dynamic_slice_in_dim(all_cotangent, start, piece.shape[1], 1)
        return total + contract(columns, piece, 1, 1)

    back = taken_in(down_proj, "fs", 1, add_cols, jnp.zeros((group_rows, hidden_cols), jnp.float32))
    grad_pre = (2.0 * jax.nn.relu(pre) * back).astype(jnp.bfloat16)

    def input_part(start, count):
        rows = lax.dynamic_slice_in_dim(grad_pre, start, count, 0)
        return contract(rows, whole_up, 1, 1)

    grad_inputs = summed_rows(input_part, inputs.shape[0], "tp")
    grad_inputs = grad_inputs.astype(jnp.bfloat16)
    shard_rows = up_proj.shape[0]

    def up_part(start, count):
        columns = lax.dynamic_slice_in_dim(all_inputs, start, count, 1)
        return contract(columns, grad_pre, 0, 0) * factor

    def down_part(start, count):
        columns = lax.dynamic_slice_in_dim(all_cotangent, start, count, 1)
        return contract(columns, active, 0, 0) * factor

    def joint_part(start, count):
        return jnp.concatenate([up_part(start, count), down_part(start, count)], axis=1)

    joint_local = summed_rows(joint_part, shard_rows, "fs")
    joint_sum = lax.psum(joint_local, "rep")
    grad_up = joint_sum[:, :hidden_cols]
    down_flip = joint_sum[:, hidden_cols:]
    grad_down = jnp.transpose(down_flip)
    energy_up = lax.psum(jnp.sum(grad_up * grad_up, axis=1), "tp") / FF
    energy_down = lax.psum(jnp.sum(grad_down * grad_down, axis=1), "fs") / D
    return (grad_inputs, grad_up, grad_down, energy_up, energy_down)


def solution(mesh):
    return jax.shard_map(
        body,
        mesh=mesh,
        in_specs=(
            P(("rep", "fs", "tp"), None),
            P("fs", "tp"),
            P("tp", "fs"),
            P(("rep", "fs", "tp"), None),
        ),
        out_specs=(P(("rep", "fs", "tp"), None), P("fs", "tp"), P("tp", "fs"), P("fs"), P("tp")),
        check_vma=False,
    )
```

profile of v0, /device:TPU:0, one launch (start us, length us, event | category | flops | bytes accessed | tf_op | source)
XLA Modules:
  0.0 594.2 jit_solution(6875754057752719887)
XLA Ops:
  7.2 0.0 all-gather.5.cloned.1.call-start
  7.2 0.7 all-gather.5.cloned.1.call-update
  7.9 0.0 all-gather.7.cloned.1.call-start
  7.9 0.7 all-gather.7.cloned.1.call-update
  8.6 0.0 all-gather.9.cloned.1.call-start
  8.7 0.7 all-gather.9.cloned.1.call-update
  9.4 0.0 all-gather.11.cloned.1.call-start
  9.4 0.5 all-gather.11.cloned.1.call-update
  10.0 0.0 reduce-scatter.5.cloned.1.call-start
  10.0 11.3 %all-gather.5.cloned.1.call-done = bf16[512,1024]{1,0:T(8,128)(2,1)} async-done(((bf16[256,1024]{1,0:T(8,128)(2,1)}), bf16[512,1024]{1,0:T(8,128)(2,1)}) %all-gather.5.cloned.1.call-update) | async-done | bytes 1048592 | tf_op jit(solution)/shard_map/all_gather | solution.py:31
  21.3 76.1 %all-gather.7.cloned.1.call-done = bf16[1024,2048]{1,0:T(8,128)(2,1)} async-done(((bf16[128,2048]{1,0:T(8,128)(2,1)}), bf16[1024,2048]{1,0:T(8,128)(2,1)}) %all-gather.7.cloned.1.call-update) | async-done | bytes 4194320 | tf_op jit(solution)/shard_map/all_gather | solution.py:36
  97.4 6.8 %fusion.2 = f32[512,2048]{1,0:T(8,128)} fusion(bf16[512,1024]{1,0:T(8,128)(2,1)} %all-gather.5.cloned.1.call-done, bf16[1024,2048]{1,0:T(8,128)(2,1)} %all-gather.7.cloned.1.call-done), kind=kOutput, calls=%fused_computation.12 | convolution fusion | flops 2147483648 | bytes 9437184 | tf_op jit(solution)/shard_map/dot_general | solution.py:37
  104.2 2.4 all-gather.9.cloned.1.call-done
  106.6 0.0 copy-start.1
  106.6 8.2 %multiply_bitcast_fusion = f32[1024,2048]{0,1:T(8,128)} fusion(bf16[512,1024]{1,0:T(8,128)(2,1)} %all-gather.9.cloned.1.call-done, f32[512,2048]{1,0:T(8,128)} %fusion.2), kind=kOutput, calls=%fused_computation.1 | convolution fusion | flops 2152726528 | bytes 13631488 | tf_op jit(solution)/shard_map/dot_general | solution.py:21
  114.8 0.0 copy-start.2
  114.8 69.5 %all-gather.11.cloned.1.call-done = bf16[2048,1024]{1,0:T(8,128)(2,1)} async-done(((bf16[2048,128]{1,0:T(8,128)(2,1)}), bf16[2048,1024]{1,0:T(8,128)(2,1)}) %all-gather.11.cloned.1.call-update) | async-done | bytes 4194320 | tf_op jit(solution)/shard_map/all_gather | solution.py:11
  184.3 0.0 copy-done.1
  184.3 5.9 multiply_convert_fusion.1
  190.2 0.0 copy-done.2
  190.2 0.0 copy-start.3
  190.2 0.0 copy-start
  190.2 2.4 multiply_bitcast_fusion.1
  192.6 0.0 copy-done.3
  192.6 1.7 copy-done
  194.3 6.4 %pad_maximum_fusion = f32[1024,4096]{0,1:T(8,128)} fusion(f32[1024,2048]{0,1:T(8,128)S(1)} %copy-done, f32[1024,2048]{0,1:T(8,128)S(1)} %multiply_bitcast_fusion.1), kind=kLoop, calls=%fused_computation | loop fusion | flops 4194304 | bytes 33554432 | tf_op jit(solution)/shard_map/concatenate | solution.py:64
  200.7 0.0 copy-start.4
  200.7 0.0 reduce-scatter.5.cloned.1.call-update
  200.8 0.0 reduce-scatter.3.cloned.1.call-start
  200.8 1.5 copy-done.4
  202.3 5.9 fusion.3
  208.2 0.0 reduce-scatter.3.cloned.1.call-update
  208.3 0.0 all-reduce.2.cloned.1.call-start
  208.3 271.0 %reduce-scatter.5.cloned.1.call-done = f32[128,4096]{0,1:T(8,128)} async-done(((f32[1024,4096]{0,1:T(8,128)}), f32[128,4096]{0,1:T(8,128)}) %reduce-scatter.5.cloned.1.call-update) | async-done | bytes 2097168 | tf_op jit(solution)/shard_map/reduce_scatter | solution.py:17
  479.3 0.0 all-reduce.2.cloned.1.call-update
  479.4 11.0 %reduce-scatter.3.cloned.1.call-done = f32[256,1024]{1,0:T(8,128)} async-done(((f32[512,1024]{1,0:T(8,128)}), f32[256,1024]{1,0:T(8,128)}) %reduce-scatter.3.cloned.1.call-update) | async-done | bytes 1048592 | tf_op jit(solution)/shard_map/reduce_scatter | solution.py:17
  490.3 2.1 convert_element_type.10
  492.4 64.5 %all-reduce.2.cloned.1.call-done = f32[128,4096]{0,1:T(8,128)} async-done(((f32[128,4096]{0,1:T(8,128)}), f32[128,4096]{0,1:T(8,128)}) %all-reduce.2.cloned.1.call-update) | async-done | bytes 2097168 | tf_op jit(solution)/shard_map/psum | solution.py:67
  556.9 2.4 multiply_reduce_fusion
  559.3 21.7 %psum.23 = f32[2048]{0:T(1024)S(1)} all-reduce(f32[2048]{0:T(1024)S(1)} %get-tuple-element.10), channel_id=1, replica_groups=mesh['rep'=2,'fs'=8,'tp'=2] {'fs'}, use_global_device_ids=true, to_apply=%region_6.7 | all-reduce | flops 2048 | bytes 16384 | tf_op jit(solution)/shard_map/psum | solution.py:72
  581.0 0.6 broadcast_multiply_fusion
  581.6 1.5 multiply_reduce_fusion.1
  583.1 2.5 psum.22
  585.6 0.5 broadcast_multiply_fusion.1
  586.1 1.3 copy.9
Async XLA Ops:
  7.2 14.1 %all-gather.5.cloned.1.call-start = ((), (), s32[]{:S(2)}) async-start(), calls=%async_computation.2 | async-start | bytes 1572864 | tf_op jit(solution)/shard_map/all_gather | solution.py:31
  7.9 89.5 %all-gather.7.cloned.1.call-start = ((), (), s32[]{:S(2)}) async-start(), calls=%async_computation.3 | async-start | bytes 4718592 | tf_op jit(solution)/shard_map/all_gather | solution.py:36
  8.6 97.9 %all-gather.9.cloned.1.call-start = ((), (), s32[]{:S(2)}) async-start(), calls=%async_computation.4 | async-start | bytes 1572864 | tf_op jit(solution)/shard_map/all_gather | solution.py:32
  9.4 174.9 %all-gather.11.cloned.1.call-start = ((), (), s32[]{:S(2)}) async-start(), calls=%async_computation.5 | async-start | bytes 4718592 | tf_op jit(solution)/shard_map/all_gather | solution.py:11
  10.0 469.4 %reduce-scatter.5.cloned.1.call-start = ((), (), s32[]{:S(2)}) async-start(), calls=%async_computation.7 | async-start | bytes 18874368 | tf_op jit(solution)/shard_map/reduce_scatter | solution.py:17
  106.6 77.7 %copy-start.1 = (bf16[512,1024]{1,0:T(8,128)(2,1)S(1)}, bf16[512,1024]{1,0:T(8,128)(2,1)}, u32[]{:S(2)}) copy-start(bf16[512,1024]{1,0:T(8,128)(2,1)} %all-gather.9.cloned.1.call-done) | copy-start | bytes 3145732
  114.8 75.4 %copy-start.2 = (bf16[512,1024]{1,0:T(8,128)(2,1)S(1)}, bf16[512,1024]{1,0:T(8,128)(2,1)}, u32[]{:S(2)}) copy-start(bf16[512,1024]{1,0:T(8,128)(2,1)} %all-gather.5.cloned.1.call-done) | copy-start | bytes 3145732
  190.2 2.4 copy-start.3
  190.2 4.1 copy-start
  200.7 1.6 copy-start.4
  200.8 289.6 %reduce-scatter.3.cloned.1.call-start = ((), (), s32[]{:S(2)}) async-start(), calls=%async_computation.6 | async-start | bytes 3145728 | tf_op jit(solution)/shard_map/reduce_scatter | solution.py:17
  208.3 348.7 %all-reduce.2.cloned.1.call-start = ((), (), s32[]{:S(2)}) async-start(), calls=%async_computation.8 | async-start | bytes 4194304 | tf_op jit(solution)/shard_map/psum | solution.py:67
Sparse Core Ops, SparseCore 0:
  9.5 11.7 all-gather.4
  23.4 73.9 all-gather.6
  99.0 7.5 all-gather.8
  108.5 75.7 all-gather.10
  200.9 278.4 reduce-scatter.4
  481.4 8.8 reduce-scatter.2
  492.6 64.2 all-reduce.1
where the time goes:
time: 595 us; the launch traced here: 594 us
  waiting for transfers between devices  508 us (85%)
  matrix products  29.2 us (5%)
  blocking collectives  24.1 us (4%)
  between operations  14.2 us (2%)
  other arithmetic  13.5 us (2%)
    reduce_scatter x2, waiting for transfers between devices, summed_rows(): return lax.psum_scatter(whole, axis, scatter_dimension=0, tiled=True)  282 us
    all_gather x1, waiting for transfers between devices, body(): whole_up = lax.all_gather(up_proj, 'fs', axis=0, tiled=True)  76.1 us
    all_gather x1, waiting for transfers between devices, taken_in(): lax.all_gather(a, axis, axis=dim, tiled=True)  69.5 us
    psum x1, waiting for transfers between devices, body(): joint_sum = lax.psum(joint_local, 'rep')  64.5 us
    dot_general x4, matrix products, contract(): lax.dot_general(left, right, (((left_dim,), (right_dim,)), ((), ())), pre...  22.4 us
    psum x1, blocking collectives, body(): energy_down = lax.psum(jnp.sum(grad_down * grad_down, axis=1), 'fs') / D  21.7 us
  transfers between devices with their start and end apart: 7, of which 7 were waited for; matrix products, arithmetic and copies ran while one was open for 4% of the time, Pallas kernels for 0%

commit v1 on v0

--- a/solution.py
+++ b/solution.py
@@ -2,6 +2,7 @@
 import jax.numpy as jnp
 from jax import lax
 from jax.sharding import PartitionSpec as P
+from jax.lax import axis_index, ppermute, psum
 
 D = 1024
 FF = 4096
@@ -33,7 +34,26 @@
     )
     hidden_cols = up_proj.shape[1]
     group_rows = all_inputs.shape[0]
-    whole_up = lax.all_gather(up_proj, "fs", axis=0, tiled=True)
+    spare = psum(1, axis_name="fs")
+    inter, lower, o_now = (spare, axis_index("fs"), up_proj.shape[0])
+    xs_all = [dev_i * inter if nth == 0 else dev_i for nth, dev_i in enumerate(up_proj.shape)]
+    y_new = jnp.zeros(xs_all, up_proj.dtype)
+    whole_up = lax.dynamic_update_slice_in_dim(y_new, up_proj, lower * o_now, axis=0)
+    right_arr = passed = up_proj
+    for i in range(1, inter // 2 + 1):
+        right_arr = ppermute(
+            right_arr, axis_name="fs", perm=[(nth, (nth + 1) % inter) for nth in range(inter)]
+        )
+        whole_up = lax.dynamic_update_slice_in_dim(
+            whole_up, right_arr, (lower - i) % inter * o_now, axis=0
+        )
+        if 2 * i < inter:
+            passed = ppermute(
+                passed, axis_name="fs", perm=[(nth, (nth - 1) % inter) for nth in range(inter)]
+            )
+            whole_up = lax.dynamic_update_slice_in_dim(
+                whole_up, passed, (lower + i) % inter * o_now, axis=0
+            )
     pre = jnp.dot(all_inputs, whole_up, preferred_element_type=jnp.float32)
     active = jnp.square(jax.nn.relu(pre)).astype(jnp.bfloat16)
 

time: 595 us -> 553 us (0.929)
  waiting for transfers between devices: 508 us -> 440 us
  starting transfers between devices: 0.27 us -> 17.6 us
  local copies, waits for them, and re-layouts: 4.54 us -> 14.2 us
    ppermute x0 -> x7, waiting for transfers between devices: none -> 82.9 us  [the longest x4 82.9 us: body(): ppermute(right_arr, axis_name='fs', perm=[(nth, (nth + 1) % inter) for nt...]
    all_gather x1 -> x0, waiting for transfers between devices: 76.1 us -> none  [body(): whole_up = lax.all_gather(up_proj, 'fs', axis=0, tiled=True)]
    all_gather x1, waiting for transfers between devices: 69.5 us -> 7.24 us  [taken_in(): lax.all_gather(a, axis, axis=dim, tiled=True)]
    ppermute x0 -> x7, starting transfers between devices: none -> 17.1 us  [the longest x3 9.23 us: body(): ppermute(passed, axis_name='fs', perm=[(nth, (nth - 1) % inter) for nth i...]
    all_gather x1, waiting for transfers between devices: 11.3 us -> 0.01 us  [body(): lax.all_gather(inputs, 'tp', axis=0, tiled=True)]
    dynamic_update_slice x0 -> x8, local copies, waits for them, and re-layouts: none -> 6.72 us  [the longest x4 3.36 us: body(): lax.dynamic_update_slice_in_dim(whole_up, right_arr, (lower - i) % inter...]
  transfers between devices with their start and end apart: 7 -> 13, of which waited for: 7 -> 8; matrix products, arithmetic and copies ran while one was open for 4% -> 6% of each run, Pallas kernels for 0% -> 0%
where the time goes in v1:
time: 553 us; the launch traced here: 552 us
  waiting for transfers between devices  440 us (80%)
  matrix products  29.2 us (5%)
  blocking collectives  24.1 us (4%)
  starting transfers between devices  17.6 us (3%)
  local copies, waits for them, and re-layouts  14.2 us (3%)
  between operations  14.2 us (3%)
  other arithmetic  13.5 us (2%)
    reduce_scatter x2, waiting for transfers between devices, summed_rows(): return lax.psum_scatter(whole, axis, scatter_dimension=0, tiled=True)  283 us
    ppermute x4, waiting for transfers between devices, body(): ppermute(right_arr, axis_name='fs', perm=[(nth, (nth + 1) % inter) for nt...  82.9 us
    psum x1, waiting for transfers between devices, body(): joint_sum = lax.psum(joint_local, 'rep')  64.3 us
    dot_general x4, matrix products, contract(): lax.dot_general(left, right, (((left_dim,), (right_dim,)), ((), ())), pre...  22.4 us
    psum x1, blocking collectives, body(): energy_down = lax.psum(jnp.sum(grad_down * grad_down, axis=1), 'fs') / D  21.7 us
  transfers between devices with their start and end apart: 13, of which 8 were waited for; matrix products, arithmetic and copies ran while one was open for 6% of the time, Pallas kernels for 0%

profile of v1, /device:TPU:0, one launch (start us, length us, event | category | flops | bytes accessed | tf_op | source)
XLA Modules:
  0.0 552.4 jit_solution(3518960255673162978)
XLA Ops:
  7.2 0.7 all-gather.4.cloned.1.call-update
  7.9 0.0 all-gather.6.cloned.1.call-start
  8.0 0.7 all-gather.6.cloned.1.call-update
  8.7 0.0 all-gather.8.cloned.1.call-start
  8.7 0.7 all-gather.8.cloned.1.call-update
  9.4 0.0 reduce-scatter.5.cloned.1.call-start
  9.4 3.0 collective-permute-start
  12.5 3.1 collective-permute-start.1
  15.6 19.6 %collective-permute-done = bf16[128,2048]{1,0:T(8,128)(2,1)S(1)} collective-permute-done((bf16[128,2048]{1,0:T(8,128)(2,1)}, bf16[128,2048]{1,0:T(8,128)(2,1)S(1)}, u32[]{:S(2)}, u32[]{:S(2)}) %collective-permute-start) | collective-permute-done | bytes 524320 | tf_op jit(solution)/shard_map/ppermute | solution.py:44
  35.2 2.4 collective-permute-start.2
  37.6 3.0 collective-permute-start.3
  40.6 2.5 broadcast_in_dim.3
  43.1 0.8 constant_dynamic-update-slice_fusion.7
  44.0 20.8 %collective-permute-done.2 = bf16[128,2048]{1,0:T(8,128)(2,1)S(1)} collective-permute-done((bf16[128,2048]{1,0:T(8,128)(2,1)S(1)}, bf16[128,2048]{1,0:T(8,128)(2,1)S(1)}, u32[]{:S(2)}, u32[]{:S(2)}) %collective-permute-start.2) | collective-permute-done | bytes 524320 | tf_op jit(solution)/shard_map/ppermute | solution.py:44
  64.8 2.5 collective-permute-start.4
  67.3 0.8 constant_dynamic-update-slice_fusion.6
  68.1 0.8 constant_dynamic-update-slice_fusion.5
  68.9 3.1 collective-permute-start.5
  72.0 0.8 constant_dynamic-update-slice_fusion.4
  72.9 18.5 %collective-permute-done.4 = bf16[128,2048]{1,0:T(8,128)(2,1)S(1)} collective-permute-done((bf16[128,2048]{1,0:T(8,128)(2,1)S(1)}, bf16[128,2048]{1,0:T(8,128)(2,1)S(1)}, u32[]{:S(2)}, u32[]{:S(2)}) %collective-permute-start.4) | collective-permute-done | bytes 524320 | tf_op jit(solution)/shard_map/ppermute | solution.py:44
  91.3 0.8 constant_dynamic-update-slice_fusion.3
  92.2 0.8 constant_dynamic-update-slice_fusion.2
  93.0 0.8 constant_dynamic-update-slice_fusion.1
  93.9 24.0 %collective-permute-done.6 = bf16[128,2048]{1,0:T(8,128)(2,1)S(1)} collective-permute-done((bf16[128,2048]{1,0:T(8,128)(2,1)S(1)}, bf16[128,2048]{1,0:T(8,128)(2,1)S(1)}, u32[]{:S(2)}, u32[]{:S(2)}) %collective-permute-start.6) | collective-permute-done | bytes 524320 | tf_op jit(solution)/shard_map/ppermute | solution.py:44
  117.9 0.8 constant_dynamic-update-slice_fusion
  118.7 6.8 %fusion.3 = f32[2048,512]{1,0:T(8,128)} fusion(bf16[1024,2048]{1,0:T(8,128)(2,1)} %constant_dynamic-update-slice_fusion, bf16[512,1024]{1,0:T(8,128)(2,1)} %all-gather.4.cloned.1.call-done), kind=kOutput, calls=%fused_computation.21 | convolution fusion | flops 2147483648 | bytes 9437184 | tf_op jit(solution)/shard_map/dot_general | solution.py:57
  125.5 8.1 %multiply_bitcast_fusion = f32[1024,2048]{0,1:T(8,128)} fusion(bf16[512,1024]{1,0:T(8,128)(2,1)} %all-gather.6.cloned.1.call-done, f32[2048,512]{1,0:T(8,128)} %fusion.3), kind=kOutput, calls=%fused_computation.1 | convolution fusion | flops 2152726528 | bytes 13631488 | tf_op jit(solution)/shard_map/dot_general | solution.py:22
  133.7 7.2 %all-gather.8.cloned.1.call-done = bf16[2048,1024]{1,0:T(8,128)(2,1)} async-done(((bf16[2048,128]{1,0:T(8,128)(2,1)}), bf16[2048,1024]{1,0:T(8,128)(2,1)}) %all-gather.8.cloned.1.call-update) | async-done | bytes 4194320 | tf_op jit(solution)/shard_map/all_gather | solution.py:12
  140.9 6.0 %fusion = bf16[512,2048]{0,1:T(8,128)(2,1)S(1)} fusion(f32[2048,512]{1,0:T(8,128)} %fusion.3, bf16[512,1024]{1,0:T(8,128)(2,1)S(1)} %copy-done.1, bf16[2048,1024]{1,0:T(8,128)(2,1)} %all-gather.8.cloned.1.call-done), kind=kOutput, calls=%fused_computation.4 | convolution fusion | flops 2151677952 | bytes 11534336 | tf_op jit(solution)/shard_map/dot_general | solution.py:22
  146.9 1.3 copy-done.4
  148.2 2.4 multiply_bitcast_fusion.1
  150.6 1.0 copy-done
  151.6 6.4 %pad_maximum_fusion = f32[1024,4096]{0,1:T(8,128)} fusion(f32[1024,2048]{0,1:T(8,128)S(1)} %copy-done, f32[1024,2048]{0,1:T(8,128)S(1)} %multiply_bitcast_fusion.1), kind=kLoop, calls=%fused_computation | loop fusion | flops 4194304 | bytes 33554432 | tf_op jit(solution)/shard_map/concatenate | solution.py:84
  158.0 0.2 reduce-scatter.3.cloned.1.call-start
  158.2 1.3 copy-done.5
  159.6 5.9 %fusion.4 = f32[512,1024]{1,0:T(8,128)} fusion(bf16[512,2048]{0,1:T(8,128)(2,1)S(1)} %copy-done.5, bf16[1024,2048]{1,0:T(8,128)(2,1)} %constant_dynamic-update-slice_fusion), kind=kOutput, calls=%fused_computation.22 | convolution fusion | flops 2147483648 | bytes 8388608 | tf_op jit(solution)/shard_map/dot_general | solution.py:22
  165.5 0.0 all-reduce.2.cloned.1.call-start
  165.5 272.1 %reduce-scatter.5.cloned.1.call-done = f32[128,4096]{0,1:T(8,128)} async-done(((f32[1024,4096]{0,1:T(8,128)}), f32[128,4096]{0,1:T(8,128)}) %reduce-scatter.5.cloned.1.call-update) | async-done | bytes 2097168 | tf_op jit(solution)/shard_map/reduce_scatter | solution.py:18
  437.6 11.0 %reduce-scatter.3.cloned.1.call-done = f32[256,1024]{1,0:T(8,128)} async-done(((f32[512,1024]{1,0:T(8,128)}), f32[256,1024]{1,0:T(8,128)}) %reduce-scatter.3.cloned.1.call-update) | async-done | bytes 1048592 | tf_op jit(solution)/shard_map/reduce_scatter | solution.py:18
  448.6 2.1 convert_element_type.11
  450.7 64.3 %all-reduce.2.cloned.1.call-done = f32[128,4096]{0,1:T(8,128)} async-done(((f32[128,4096]{0,1:T(8,128)}), f32[128,4096]{0,1:T(8,128)}) %all-reduce.2.cloned.1.call-update) | async-done | bytes 2097168 | tf_op jit(solution)/shard_map/psum | solution.py:87
  515.0 2.4 multiply_reduce_fusion
  517.4 21.7 %psum.23 = f32[2048]{0:T(1024)S(1)} all-reduce(f32[2048]{0:T(1024)S(1)} %get-tuple-element.10), channel_id=1, replica_groups=mesh['rep'=2,'fs'=8,'tp'=2] {'fs'}, use_global_device_ids=true, to_apply=%region_6.7 | all-reduce | flops 2048 | bytes 16384 | tf_op jit(solution)/shard_map/psum | solution.py:92
  539.1 0.6 broadcast_multiply_fusion
  539.7 1.5 multiply_reduce_fusion.1
  541.2 2.5 psum.22
  543.7 0.5 broadcast_multiply_fusion.1
  544.2 1.3 copy.10
  (19 shorter events, 0.1 us)
Async XLA Ops:
  7.2 35.9 %copy-start.2 = (bf16[128,2048]{1,0:T(8,128)(2,1)S(1)}, bf16[128,2048]{1,0:T(8,128)(2,1)}, u32[]{:S(2)}) copy-start(bf16[128,2048]{1,0:T(8,128)(2,1)} %param.5) | copy-start | bytes 1572868
  7.2 111.5 %all-gather.4.cloned.1.call-start = ((), (), s32[]{:S(2)}) async-start(), calls=%async_computation.2 | async-start | bytes 1572864 | tf_op jit(solution)/shard_map/all_gather | solution.py:32
  7.9 117.6 %all-gather.6.cloned.1.call-start = ((), (), s32[]{:S(2)}) async-start(), calls=%async_computation.3 | async-start | bytes 1572864 | tf_op jit(solution)/shard_map/all_gather | solution.py:33
  8.7 132.2 %all-gather.8.cloned.1.call-start = ((), (), s32[]{:S(2)}) async-start(), calls=%async_computation.4 | async-start | bytes 4718592 | tf_op jit(solution)/shard_map/all_gather | solution.py:12
  9.4 428.2 %reduce-scatter.5.cloned.1.call-start = ((), (), s32[]{:S(2)}) async-start(), calls=%async_computation.6 | async-start | bytes 18874368 | tf_op jit(solution)/shard_map/reduce_scatter | solution.py:18
  9.4 25.8 %collective-permute-start = (bf16[128,2048]{1,0:T(8,128)(2,1)}, bf16[128,2048]{1,0:T(8,128)(2,1)S(1)}, u32[]{:S(2)}, u32[]{:S(2)}) collective-permute-start(bf16[128,2048]{1,0:T(8,128)(2,1)} %param.5), channel_id=1, source_target_pairs={{0,2},{2,4},{4,6},{6,8},{8,10},{10,12},{12,14},{14,0},{1,3},{3,5},... | collective-permute-start | bytes 1572872 | tf_op jit(solution)/shard_map/ppermute | solution.py:44
  12.5 25.1 %collective-permute-start.1 = (bf16[128,2048]{1,0:T(8,128)(2,1)}, bf16[128,2048]{1,0:T(8,128)(2,1)S(1)}, u32[]{:S(2)}, u32[]{:S(2)}) collective-permute-start(bf16[128,2048]{1,0:T(8,128)(2,1)} %param.5), channel_id=1, source_target_pairs={{0,14},{2,0},{4,2},{6,4},{8,6},{10,8},{12,10},{14,12},{1,15},{3,1}... | collective-permute-start | bytes 1572872 | tf_op jit(solution)/shard_map/ppermute | solution.py:51
  35.2 29.6 %collective-permute-start.2 = (bf16[128,2048]{1,0:T(8,128)(2,1)S(1)}, bf16[128,2048]{1,0:T(8,128)(2,1)S(1)}, u32[]{:S(2)}, u32[]{:S(2)}) collective-permute-start(bf16[128,2048]{1,0:T(8,128)(2,1)S(1)} %collective-permute-done), channel_id=1, source_target_pairs={{0,2},{2,4},{4,6},{6,8},{8,10},{10,12},{12,14},{14,0},{1,3},{3,5},... | collective-permute-start | bytes 1572872 | tf_op jit(solution)/shard_map/ppermute | solution.py:44
  37.6 31.3 %collective-permute-start.3 = (bf16[128,2048]{1,0:T(8,128)(2,1)S(1)}, bf16[128,2048]{1,0:T(8,128)(2,1)S(1)}, u32[]{:S(2)}, u32[]{:S(2)}) collective-permute-start(bf16[128,2048]{1,0:T(8,128)(2,1)S(1)} %collective-permute-done.1), channel_id=1, source_target_pairs={{0,14},{2,0},{4,2},{6,4},{8,6},{10,8},{12,10},{14,12},{1,15},{3,1}... | collective-permute-start | bytes 1572872 | tf_op jit(solution)/shard_map/ppermute | solution.py:51
  64.8 26.5 %collective-permute-start.4 = (bf16[128,2048]{1,0:T(8,128)(2,1)S(1)}, bf16[128,2048]{1,0:T(8,128)(2,1)S(1)}, u32[]{:S(2)}, u32[]{:S(2)}) collective-permute-start(bf16[128,2048]{1,0:T(8,128)(2,1)S(1)} %collective-permute-done.2), channel_id=1, source_target_pairs={{0,2},{2,4},{4,6},{6,8},{8,10},{10,12},{12,14},{14,0},{1,3},{3,5},... | collective-permute-start | bytes 1572872 | tf_op jit(solution)/shard_map/ppermute | solution.py:44
  68.9 24.1 %collective-permute-start.5 = (bf16[128,2048]{1,0:T(8,128)(2,1)S(1)}, bf16[128,2048]{1,0:T(8,128)(2,1)S(1)}, u32[]{:S(2)}, u32[]{:S(2)}) collective-permute-start(bf16[128,2048]{1,0:T(8,128)(2,1)S(1)} %collective-permute-done.3), channel_id=1, source_target_pairs={{0,14},{2,0},{4,2},{6,4},{8,6},{10,8},{12,10},{14,12},{1,15},{3,1}... | collective-permute-start | bytes 1572872 | tf_op jit(solution)/shard_map/ppermute | solution.py:51
  91.3 26.6 %collective-permute-start.6 = (bf16[128,2048]{1,0:T(8,128)(2,1)S(1)}, bf16[128,2048]{1,0:T(8,128)(2,1)S(1)}, u32[]{:S(2)}, u32[]{:S(2)}) collective-permute-start(bf16[128,2048]{1,0:T(8,128)(2,1)S(1)} %collective-permute-done.4), channel_id=1, source_target_pairs={{0,2},{2,4},{4,6},{6,8},{8,10},{10,12},{12,14},{14,0},{1,3},{3,5},... | collective-permute-start | bytes 1572872 | tf_op jit(solution)/shard_map/ppermute | solution.py:44
  125.5 15.4 %copy-start.1 = (bf16[512,1024]{1,0:T(8,128)(2,1)S(1)}, bf16[512,1024]{1,0:T(8,128)(2,1)}, u32[]{:S(2)}) copy-start(bf16[512,1024]{1,0:T(8,128)(2,1)} %all-gather.6.cloned.1.call-done) | copy-start | bytes 3145732
  133.7 14.5 %copy-start.3 = (bf16[512,1024]{1,0:T(8,128)(2,1)S(1)}, bf16[512,1024]{1,0:T(8,128)(2,1)}, u32[]{:S(2)}) copy-start(bf16[512,1024]{1,0:T(8,128)(2,1)} %all-gather.4.cloned.1.call-done) | copy-start | bytes 3145732
  146.9 1.3 copy-start.4
  148.2 3.4 copy-start
  158.0 1.6 copy-start.5
  158.0 290.6 %reduce-scatter.3.cloned.1.call-start = ((), (), s32[]{:S(2)}) async-start(), calls=%async_computation.5 | async-start | bytes 3145728 | tf_op jit(solution)/shard_map/reduce_scatter | solution.py:18
  165.5 349.6 %all-reduce.2.cloned.1.call-start = ((), (), s32[]{:S(2)}) async-start(), calls=%async_computation.7 | async-start | bytes 4194304 | tf_op jit(solution)/shard_map/psum | solution.py:87
Sparse Core Ops, SparseCore 0:
  9.5 11.7 all-gather.3
  22.9 10.1 all-gather.5
  35.1 105.7 all-gather.7
  158.1 279.4 reduce-scatter.4
  439.7 8.8 reduce-scatter.2
  450.8 64.2 all-reduce.1
